TPU v7x, 32 devices: a whole 2x2x4 slice. The times are simulated.
32 devices in a mesh: sp: 8 (over z, x), tp: 4 (over y, core).
Axes of the slice: x: 2, y: 2, z: 4, core: 2. Of those that a mesh axis runs over, the one named last changes fastest.
Arguments:
- queries: bfloat16 [2048, 1024], P('sp', 'tp'), may hold values from -6 to 6
- keys: bfloat16 [2048, 256], P('sp'), may hold values from -6 to 6
- values: bfloat16 [2048, 256], P('sp'), may hold values from -6 to 6
- sink: float32 [16], P('tp'), may hold values from 3 to 6
- w_out: bfloat16 [1024, 2048], P('tp'), may hold values from -0.1875 to 0.1875
- stream: bfloat16 [2048, 2048], P(('sp', 'tp')), may hold values from -6 to 6
- gain: bfloat16 [2048], replicated, may hold values from 0.099609375 to 1.8984375
- routes: int32 [2048, 4], P('sp'), may hold values from 0 to 63, all different within a row; in each aligned block of 64 rows (0 to 63, 64 to 127, ...) at most 8 rows name the same one
- route_weights: float32 [2048, 4], P('sp'), may hold values from 0.2 to 1
- w_gate: bfloat16 [64, 1024, 2048], P('sp', 'tp'), may hold values from -0.125 to 0.125
- w_up: bfloat16 [64, 1024, 2048], P('sp', 'tp'), may hold values from -0.125 to 0.125
- w_down: bfloat16 [64, 1024, 2048], P('sp', None, 'tp'), may hold values from -0.1875 to 0.1875
- shared_gate: bfloat16 [1024, 2048], P('tp'), may hold values from -0.125 to 0.125
- shared_up: bfloat16 [1024, 2048], P('tp'), may hold values from -0.125 to 0.125
- shared_down: bfloat16 [1024, 2048], P(None, 'tp'), may hold values from -0.1875 to 0.1875
Outputs:
- layer_out: bfloat16 [2048, 2048], P('sp', 'tp')
Inputs may be any that keep to these rules, and one draw needn't show every extreme that they name: `routes`: in each aligned block of 64 rows no expert is named in more than 8 rows, and some blocks reach 8; a row names 4 different experts.
All inputs are finite; a program needn't handle non-finite values.
Results may differ from a plain program's by a relative error of at most 0.014.
Values may be sent and summed in bfloat16 or wider, within the bound.
A program may use at most 128 MiB of HBM per device.

v0:
```python
import jax
import jax.numpy as jnp
from jax import lax
from jax.sharding import PartitionSpec as P

D = 2048
HEADS = 16
KV_HEADS = 4
HD = 64
WINDOW = 128
EXPERTS = 64
TOPK = 4
NORM_EPS = 1e-05


def with_halo(array, sides, width):
    for axis, dim in sides:
        devices, length = (lax.axis_size(axis), array.shape[dim])
        up = [(i, (i + 1) % devices) for i in range(devices - 1)]
        down = [(j, i) for i, j in up]
        last = lax.slice_in_dim(array, length - width, length, axis=dim)
        leading = lax.slice_in_dim(array, 0, width, axis=dim)
        before = lax.ppermute(last, axis, up)
        after = lax.ppermute(leading, axis, down)
        array = jnp.concatenate([before, array, after], axis=dim)
    return array


def slot_ids(block_routes, capacity):
    flat_routes = block_routes.reshape(-1)
    hit_table = (flat_routes[:, None] == jnp.arange(EXPERTS)[None, :]).astype(jnp.int32)
    earlier = jnp.cumsum(hit_table, axis=0) - hit_table
    slot_rank = jnp.sum(earlier * hit_table, axis=1)
    return flat_routes * capacity + slot_rank


def local(
    queries,
    keys,
    values,
    sink,
    w_out,
    stream,
    gain,
    routes,
    route_weights,
    w_gate,
    w_up,
    w_down,
    shared_gate,
    shared_up,
    shared_down,
):
    tok_dev = queries.shape[0]
    n_tp = lax.axis_size("tp")
    n_sp = lax.axis_size("sp")
    tp_idx = lax.axis_index("tp")
    sp_idx = lax.axis_index("sp")
    heads_dev = HEADS // n_tp
    group = HEADS // KV_HEADS
    kv_head = tp_idx * heads_dev // group
    key_own = lax.dynamic_slice_in_dim(keys, kv_head * HD, HD, 1)
    value_own = lax.dynamic_slice_in_dim(values, kv_head * HD, HD, 1)
    paired = jnp.concatenate([key_own, value_own], axis=1)
    padded = with_halo(paired, (("sp", 0),), WINDOW)
    blocks = tok_dev // WINDOW
    framed = padded.reshape(blocks + 2, WINDOW, 2 * HD)
    banded = jnp.concatenate([framed[:-2], framed[1:-1], framed[2:]], axis=1)
    key_band = banded[:, :, :HD]
    value_band = banded[:, :, HD:]
    query_blocks = queries.reshape(blocks, WINDOW, heads_dev, HD)
    scores = jnp.einsum(
        "nqhd,njd->nhqj", query_blocks, key_band, preferred_element_type=jnp.float32
    ) * HD ** (-0.5)
    offset = sp_idx * tok_dev
    seq_total = tok_dev * n_sp
    query_pos = (
        offset + jnp.arange(blocks)[:, None, None] * WINDOW + jnp.arange(WINDOW)[None, :, None]
    )
    key_pos = (
        offset
        - WINDOW
        + jnp.arange(blocks)[:, None, None] * WINDOW
        + jnp.arange(3 * WINDOW)[None, None, :]
    )
    allowed = (jnp.abs(query_pos - key_pos) <= WINDOW) & (key_pos >= 0) & (key_pos < seq_total)
    scores = jnp.where(allowed[:, None], scores, -jnp.inf)
    sink_level = sink.reshape(1, heads_dev, 1, 1)
    row_peak = jnp.maximum(scores.max(-1, keepdims=True), sink_level)
    probabilities = jnp.exp(scores - row_peak)
    denominator = probabilities.sum(-1, keepdims=True) + jnp.exp(sink_level - row_peak)
    weights = (probabilities / denominator).astype(jnp.bfloat16)
    attended = jnp.einsum("nhqj,njd->nqhd", weights, value_band, preferred_element_type=jnp.float32)
    attended = attended.astype(jnp.bfloat16).reshape(tok_dev, heads_dev * HD)
    rows_dev = tok_dev // n_tp
    d_dev = w_down.shape[2]
    projected = lax.psum_scatter(
        jnp.dot(attended, w_out, preferred_element_type=jnp.float32),
        "tp",
        scatter_dimension=0,
        tiled=True,
    )
    mixed_rows = (stream.astype(jnp.float32) + projected).astype(jnp.bfloat16)
    whole_rows = lax.all_gather(mixed_rows, "tp", axis=0, tiled=True)
    wide_rows = whole_rows.astype(jnp.float32)
    scale_rows = lax.rsqrt(jnp.mean(wide_rows * wide_rows, axis=-1, keepdims=True) + NORM_EPS)
    normed = (wide_rows * scale_rows * gain.astype(jnp.float32)).astype(jnp.bfloat16)
    residual = lax.dynamic_slice_in_dim(wide_rows, tp_idx * d_dev, d_dev, 1)
    exp_dev = w_gate.shape[0]
    capacity = max(1, 2 * tok_dev * TOPK // (n_tp * EXPERTS))
    slot_count = EXPERTS * capacity
    blocked_routes = routes.reshape(n_tp, rows_dev, TOPK)
    destination = jax.vmap(lambda block_routes: slot_ids(block_routes, capacity))(blocked_routes)
    slot_select = destination[:, None, :] == jnp.arange(slot_count)[None, :, None]
    slot_select = slot_select.reshape(n_tp, slot_count, rows_dev, TOPK).astype(jnp.float32)
    dispatch_table = jnp.sum(slot_select, axis=-1).astype(jnp.bfloat16)
    combine_table = jnp.sum(slot_select * route_weights.reshape(n_tp, 1, rows_dev, TOPK), axis=-1)
    normed_blocks = normed.reshape(n_tp, rows_dev, D)
    own_table = lax.dynamic_index_in_dim(dispatch_table, tp_idx, 0, keepdims=False)
    own_rows = lax.dynamic_index_in_dim(normed_blocks, tp_idx, 0, keepdims=False)
    outgoing = jnp.dot(own_table, own_rows, preferred_element_type=jnp.float32).astype(jnp.bfloat16)
    arrived = lax.all_to_all(outgoing, "sp", split_axis=0, concat_axis=0, tiled=True)
    arrived = arrived.reshape(1, n_sp, exp_dev, capacity, D)
    piece_rows = lax.all_gather(arrived, "tp", axis=0, tiled=True)
    gate_act = jnp.einsum(
        "tsecd,efd->tsecf", piece_rows, w_gate, preferred_element_type=jnp.float32
    )
    up_act = jnp.einsum("tsecd,efd->tsecf", piece_rows, w_up, preferred_element_type=jnp.float32)
    hidden = (jax.nn.silu(gate_act) * up_act).astype(jnp.bfloat16)
    shared_gate_act = jnp.einsum(
        "td,fd->tf", normed, shared_gate, preferred_element_type=jnp.float32
    )
    shared_up_act = jnp.einsum("td,fd->tf", normed, shared_up, preferred_element_type=jnp.float32)
    shared_hidden = (jax.nn.silu(shared_gate_act) * shared_up_act).astype(jnp.bfloat16)
    shared_hidden = shared_hidden.reshape(1, 1, 1, tok_dev, shared_hidden.shape[1])
    expert_piece = lax.all_gather(hidden, "tp", axis=4, tiled=True)
    shared_piece = lax.all_gather(shared_hidden, "tp", axis=4, tiled=True)
    piece_width = expert_piece.shape[4]
    routed_total = jnp.einsum(
        "tsecf,efd->tsecd", expert_piece, w_down, preferred_element_type=jnp.float32
    )
    shared_total = jnp.dot(
        shared_piece.reshape(tok_dev, piece_width), shared_down, preferred_element_type=jnp.float32
    )
    returned = lax.all_to_all(
        routed_total.astype(jnp.bfloat16), "sp", split_axis=1, concat_axis=1, tiled=True
    )
    returned = returned.reshape(n_tp, slot_count, d_dev).astype(jnp.float32)
    routed = jnp.einsum("tmr,tmd->trd", combine_table, returned, precision=lax.Precision.HIGHEST)
    routed = routed.reshape(tok_dev, d_dev)
    return (residual + routed + shared_total).astype(jnp.bfloat16)


def solution(mesh):
    placed = (
        P("sp", "tp"),
        P("sp", None),
        P("sp", None),
        P("tp"),
        P("tp", None),
        P(("sp", "tp"), None),
        P(),
        P("sp", None),
        P("sp", None),
        P("sp", "tp", None),
        P("sp", "tp", None),
        P("sp", None, "tp"),
        P("tp", None),
        P("tp", None),
        P(None, "tp"),
    )
    return jax.shard_map(
        local, mesh=mesh, in_specs=placed, out_specs=P("sp", "tp"), check_vma=False
    )
```

profile of v0, /device:TPU:0, one launch (start us, length us, event | category | flops | bytes accessed | tf_op | source)
XLA Modules:
  0.0 317.8 jit_solution(6857469026317906916)
XLA Ops:
  7.7 4.9 %collective-permute-start = (bf16[128,128]{1,0:T(8,128)(2,1)S(1)}, bf16[128,128]{1,0:T(8,128)(2,1)S(1)}, u32[]{:S(2)}, u32[]{:S(2)}) collective-permute-start(bf16[128,128]{1,0:T(8,128)(2,1)S(1)} %get-tuple-element.10), channel_id=1, source_target_pairs={{0,4},{4,8},{8,12},{12,16},{16,20},{20,24},{24,28},{1,5},{5,9},{9,... | collective-permute-start | bytes 98312 | tf_op jit(solution)/shard_map/ppermute | solution.py:23
  12.6 1.3 collective-permute-start.1
  15.7 2.7 collective-permute-done.1
  20.4 1.8 fusion.27
  22.3 32.5 %reduce-scatter.2.cloned.1.call-done = f32[64,2048]{1,0:T(8,128)} async-done(((f32[256,2048]{1,0:T(8,128)}), f32[64,2048]{1,0:T(8,128)}) %reduce-scatter.2.cloned.1.call-update) | async-done | bytes 524304 | tf_op jit(solution)/shard_map/reduce_scatter | solution.py:97
  54.7 1.8 add_convert_fusion
  57.2 2.4 reduce-window.6
  60.4 1.3 convert_reduce_fusion
  61.7 11.7 %all-gather.5.cloned.1.call-done = bf16[256,2048]{1,0:T(8,128)(2,1)} async-done(((bf16[64,2048]{1,0:T(8,128)(2,1)}), bf16[256,2048]{1,0:T(8,128)(2,1)}) %all-gather.5.cloned.1.call-update) | async-done | bytes 1048592 | tf_op jit(solution)/shard_map/all_gather | solution.py:104
  73.4 1.5 multiply_reduce_fusion
  74.9 1.5 multiply_convert_fusion
  77.2 53.9 %all_to_all.14 = bf16[8,64,2048]{2,1,0:T(8,128)(2,1)S(1)} all-to-all(bf16[8,64,2048]{2,1,0:T(8,128)(2,1)S(1)} %bitcast.114), channel_id=1, replica_groups=mesh['sp'=8,'tp'=4] {'sp'}, dimensions={0} | all-to-all | bytes 4194304 | tf_op jit(solution)/shard_map/all_to_all | solution.py:122
  131.1 1.5 copy.68
  132.8 56.3 %all-gather.7.cloned.1.call-done = bf16[4,8,8,8,2048]{4,3,1,0,2:T(8,128)(2,1)} async-done(((bf16[1,8,8,8,2048]{4,3,1,0,2:T(8,128)(2,1)}), bf16[4,8,8,8,2048]{4,3,1,0,2:T(8,128)(2,1)}) %all-gather.7.cloned.1.call-update) | async-done | bytes 8388624 | tf_op jit(solution)/shard_map/all_gather | solution.py:124
  189.2 8.1 %fusion.4 = f32[8,4,8,8,256]{4,3,2,1,0:T(8,128)S(1)} fusion(bf16[4,8,8,8,2048]{4,3,1,0,2:T(8,128)(2,1)} %all-gather.7.cloned.1.call-done, bf16[8,256,2048]{2,1,0:T(8,128)(2,1)} %param.24), kind=kOutput, calls=%fused_computation.4 | convolution fusion | flops 2147483648 | bytes 18874368 | tf_op jit(solution)/shard_map/tsecd,efd->tsecf/dot_general | solution.py:125
  197.3 11.4 %fusion.6 = bf16[4,8,8,8,256]{4,3,1,0,2:T(8,128)(2,1)} fusion(f32[8,4,8,8,256]{4,3,2,1,0:T(8,128)S(1)} %fusion.4, bf16[4,8,8,8,2048]{4,3,1,0,2:T(8,128)(2,1)} %all-gather.7.cloned.1.call-done, bf16[8,256,2048]{2,1,0:T(8,128)(2,1)} %param.25), kind=kOutput, calls=%fused_computation.8 | convolution fusion | flops 2150629376 | bytes 19922944 | tf_op jit(solution)/shard_map/tsecd,efd->tsecf/dot_general | solution.py:128
  208.7 35.2 %all-gather.9.cloned.1.call-done = bf16[4,8,8,8,1024]{4,3,1,0,2:T(8,128)(2,1)} async-done(((bf16[4,8,8,8,256]{4,3,1,0,2:T(8,128)(2,1)}), bf16[4,8,8,8,1024]{4,3,1,0,2:T(8,128)(2,1)}) %all-gather.9.cloned.1.call-update) | async-done | bytes 4194320 | tf_op jit(solution)/shard_map/all_gather | solution.py:136
  243.8 7.0 %convert_bitcast_fusion = bf16[4,8,8,8,512]{4,3,1,0,2:T(8,128)(2,1)S(1)} fusion(bf16[4,8,8,8,1024]{4,3,1,0,2:T(8,128)(2,1)} %all-gather.9.cloned.1.call-done, bf16[8,1024,512]{2,1,0:T(8,128)(2,1)} %param.26), kind=kOutput, calls=%fused_computation.14 | convolution fusion | flops 2148532224 | bytes 14680064 | tf_op jit(solution)/shard_map/tsecf,efd->tsecd/dot_general | solution.py:139
  250.8 1.6 copy.69
  252.4 5.6 %all-to-all-start.1 = ((bf16[4,8,8,8,512]{4,3,0,2,1:T(8,128)(2,1)}), bf16[4,8,8,8,512]{4,3,0,2,1:T(8,128)(2,1)S(1)}, u32[]{:S(2)}, u32[]{:S(2)}) async-start(bf16[4,8,8,8,512]{4,3,0,2,1:T(8,128)(2,1)} %copy.69), calls=%async_computation.2 | async-start | bytes 4194304 | tf_op jit(solution)/shard_map/all_to_all | solution.py:145
  258.1 1.6 convert_element_type.61
  261.3 7.4 %all-gather = bf16[256,1024]{1,0:T(8,128)(2,1)} all-gather(bf16[256,256]{1,0:T(8,128)(2,1)S(1)} %fusion.16), channel_id=2, replica_groups=mesh['sp'=8,'tp'=4] {'tp'}, dimensions={1}, use_global_device_ids=true | all-gather | bytes 655360 | tf_op jit(solution)/shard_map/all_gather | solution.py:137
  268.7 38.0 %all-to-all-done.1 = bf16[4,8,8,8,512]{4,3,0,2,1:T(8,128)(2,1)S(1)} async-done(((bf16[4,8,8,8,512]{4,3,0,2,1:T(8,128)(2,1)}), bf16[4,8,8,8,512]{4,3,0,2,1:T(8,128)(2,1)S(1)}, u32[]{:S(2)}, u32[]{:S(2)}) %all-to-all-start.1) | async-done | bytes 2097184 | tf_op jit(solution)/shard_map/all_to_all | solution.py:145
  307.8 1.2 fusion.42
  (84 shorter events, 12.3 us)
Async XLA Ops:
  6.5 13.8 %copy-start = (bf16[256,2048]{1,0:T(8,128)(2,1)S(1)}, bf16[256,2048]{1,0:T(8,128)(2,1)}, u32[]{:S(2)}) copy-start(bf16[256,2048]{1,0:T(8,128)(2,1)} %param.19) | copy-start | bytes 3145732
  6.5 48.2 %reduce-scatter.2.cloned.1.call-start = ((), (), s32[]{:S(2)}) async-start(), calls=%async_computation.3 | async-start | bytes 2621440 | tf_op jit(solution)/shard_map/reduce_scatter | solution.py:97
  6.5 12.9 %copy-start.13 = (f32[4]{0:T(128)S(1)}, f32[4]{0:T(128)}, u32[]{:S(2)}) copy-start(f32[4]{0:T(128)} %param.18) | copy-start | bytes 52
  7.7 8.0 %collective-permute-start = (bf16[128,128]{1,0:T(8,128)(2,1)S(1)}, bf16[128,128]{1,0:T(8,128)(2,1)S(1)}, u32[]{:S(2)}, u32[]{:S(2)}) collective-permute-start(bf16[128,128]{1,0:T(8,128)(2,1)S(1)} %get-tuple-element.10), channel_id=1, source_target_pairs={{0,4},{4,8},{8,12},{12,16},{16,20},{20,24},{24,28},{1,5},{5,9},{9,... | collective-permute-start | bytes 98312 | tf_op jit(solution)/shard_map/ppermute | solution.py:23
  12.6 5.8 %collective-permute-start.1 = (bf16[128,128]{1,0:T(8,128)(2,1)S(1)}, bf16[128,128]{1,0:T(8,128)(2,1)S(1)}, u32[]{:S(2)}, u32[]{:S(2)}) collective-permute-start(bf16[128,128]{1,0:T(8,128)(2,1)S(1)} %get-tuple-element.11), channel_id=1, source_target_pairs={{4,0},{8,4},{12,8},{16,12},{20,16},{24,20},{28,24},{5,1},{9,5},{13... | collective-permute-start | bytes 98312 | tf_op jit(solution)/shard_map/ppermute | solution.py:24
  20.4 34.4 %copy-start.9 = (bf16[64,2048]{1,0:T(8,128)(2,1)S(1)}, bf16[64,2048]{1,0:T(8,128)(2,1)}, u32[]{:S(2)}) copy-start(bf16[64,2048]{1,0:T(8,128)(2,1)} %param.20) | copy-start | bytes 786436
  22.2 34.4 %copy-start.10 = (s32[256,4]{0,1:T(4,128)S(1)}, s32[256,4]{0,1:T(4,128)}, u32[]{:S(2)}) copy-start(s32[256,4]{0,1:T(4,128)} %param.22) | copy-start | bytes 12292
  22.2 38.1 %copy-start.11 = (f32[256,4]{0,1:T(4,128)S(1)}, f32[256,4]{0,1:T(4,128)}, u32[]{:S(2)}) copy-start(f32[256,4]{0,1:T(4,128)} %param.23) | copy-start | bytes 12292
  22.2 38.2 %copy-start.12 = (bf16[2048]{0:T(1024)(128)(2,1)S(1)}, bf16[2048]{0:T(1024)(128)(2,1)}, u32[]{:S(2)}) copy-start(bf16[2048]{0:T(1024)(128)(2,1)} %param.21) | copy-start | bytes 12292
  22.2 51.2 %all-gather.5.cloned.1.call-start = ((), (), s32[]{:S(2)}) async-start(), calls=%async_computation.4 | async-start | bytes 1310720 | tf_op jit(solution)/shard_map/all_gather | solution.py:104
  56.5 132.6 %all-gather.7.cloned.1.call-start = ((), (), s32[]{:S(2)}) async-start(), calls=%async_computation.5 | async-start | bytes 10485760 | tf_op jit(solution)/shard_map/all_gather | solution.py:124
  76.5 54.6 %copy-start.3 = (bf16[256,2048]{1,0:T(8,128)(2,1)}, bf16[256,2048]{1,0:T(8,128)(2,1)S(1)}, u32[]{:S(2)}) copy-start(bf16[256,2048]{1,0:T(8,128)(2,1)S(1)} %multiply_convert_fusion) | copy-start | bytes 3145732
  132.6 111.2 %all-gather.9.cloned.1.call-start = ((), (), s32[]{:S(2)}) async-start(), calls=%async_computation.6 | async-start | bytes 5242880 | tf_op jit(solution)/shard_map/all_gather | solution.py:136
  252.4 5.6 %copy-start.2 = (bf16[256,2048]{1,0:T(8,128)(2,1)S(1)}, bf16[256,2048]{1,0:T(8,128)(2,1)}, u32[]{:S(2)}) copy-start(bf16[256,2048]{1,0:T(8,128)(2,1)} %all-gather.5.cloned.1.call-done) | copy-start | bytes 3145732
  252.4 54.3 %all-to-all-start.1 = ((bf16[4,8,8,8,512]{4,3,0,2,1:T(8,128)(2,1)}), bf16[4,8,8,8,512]{4,3,0,2,1:T(8,128)(2,1)S(1)}, u32[]{:S(2)}, u32[]{:S(2)}) async-start(bf16[4,8,8,8,512]{4,3,0,2,1:T(8,128)(2,1)} %copy.69), calls=%async_computation.2 | async-start | bytes 4194304 | tf_op jit(solution)/shard_map/all_to_all | solution.py:145
  258.1 1.6 copy-start.4
  258.1 2.3 copy-start.7
  258.1 2.8 copy-start.14
  306.7 1.0 copy-start.6
  307.8 2.3 copy-start.5
  307.8 2.3 copy-start.8
  307.8 3.5 %copy-start.1 = (bf16[256,2048]{1,0:T(8,128)(2,1)S(1)}, bf16[256,2048]{1,0:T(8,128)(2,1)}, u32[]{:S(2)}) copy-start(bf16[256,2048]{1,0:T(8,128)(2,1)} %param.19) | copy-start | bytes 3145732
Sparse Core Ops, SparseCore 0:
  22.3 32.3 reduce-scatter.1
  56.7 16.6 all-gather.4
  132.7 56.3 all-gather.6
  208.8 34.9 all-gather.8
where the time goes:
time: 318 us
  waiting for transfers between devices  176 us (55%)
  blocking collectives  61.2 us (19%)
  matrix products  33.1 us (10%)
  between operations  13.5 us (4%)
  other arithmetic  12.7 us (4%)
  starting transfers between devices  12.1 us (4%)
  local copies, waits for them, and re-layouts  8.65 us (3%)
    all_gather x1, waiting for transfers between devices, local(): piece_rows = lax.all_gather(arrived, 'tp', axis=0, tiled=True)  56.3 us
    all_to_all x1, blocking collectives, local(): lax.all_to_all(outgoing, 'sp', split_axis=0, concat_axis=0, tiled=True)  53.9 us
    all_to_all x1, waiting for transfers between devices, local(): lax.all_to_all(routed_total.astype(jnp.bfloat16), 'sp', split_axis=1, con...  38 us
    all_gather x1, waiting for transfers between devices, local(): expert_piece = lax.all_gather(hidden, 'tp', axis=4, tiled=True)  35.2 us
    reduce_scatter x1, waiting for transfers between devices, local(): lax.psum_scatter(jnp.dot(attended, w_out, preferred_element_type=jnp.floa...  32.5 us
    all_gather x1, waiting for transfers between devices, local(): whole_rows = lax.all_gather(mixed_rows, 'tp', axis=0, tiled=True)  11.7 us
    dot_general x1, matrix products, local(): jnp.einsum('tsecd,efd->tsecf', piece_rows, w_up, preferred_element_type=j...  11.4 us
    dot_general x1, matrix products, local(): jnp.einsum('tsecd,efd->tsecf', piece_rows, w_gate, preferred_element_type...  8.13 us
  transfers between devices with their start and end apart: 7, of which 6 were waited for; matrix products, arithmetic and copies ran while one was open for 3% of the time, Pallas kernels for 0%

commit v1 on v0

--- a/solution.py
+++ b/solution.py
@@ -133,7 +133,8 @@
     shared_up_act = jnp.einsum("td,fd->tf", normed, shared_up, preferred_element_type=jnp.float32)
     shared_hidden = (jax.nn.silu(shared_gate_act) * shared_up_act).astype(jnp.bfloat16)
     shared_hidden = shared_hidden.reshape(1, 1, 1, tok_dev, shared_hidden.shape[1])
-    expert_piece = lax.all_gather(hidden, "tp", axis=4, tiled=True)
+    u_next = lax.all_gather(hidden, axis_name="tp")
+    expert_piece = jnp.concatenate(u_next, 4)
     shared_piece = lax.all_gather(shared_hidden, "tp", axis=4, tiled=True)
     piece_width = expert_piece.shape[4]
     routed_total = jnp.einsum(

time: 318 us -> 319 us (level)
  no operation moved by 1% of the time
where the time goes in v1:
time: 319 us
  waiting for transfers between devices  176 us (55%)
  blocking collectives  61.2 us (19%)
  matrix products  31.9 us (10%)
  between operations  13.5 us (4%)
  other arithmetic  12.7 us (4%)
  starting transfers between devices  12.1 us (4%)
  local copies, waits for them, and re-layouts  11.4 us (4%)
    all_gather x1, waiting for transfers between devices, local(): piece_rows = lax.all_gather(arrived, 'tp', axis=0, tiled=True)  56.3 us
    all_to_all x1, blocking collectives, local(): lax.all_to_all(outgoing, 'sp', split_axis=0, concat_axis=0, tiled=True)  53.9 us
    all_to_all x1, waiting for transfers between devices, local(): lax.all_to_all(routed_total.astype(jnp.bfloat16), 'sp', split_axis=1, con...  38 us
    all_gather x1, waiting for transfers between devices, local(): u_next = lax.all_gather(hidden, axis_name='tp')  34.6 us
    reduce_scatter x1, waiting for transfers between devices, local(): lax.psum_scatter(jnp.dot(attended, w_out, preferred_element_type=jnp.floa...  32.5 us
    all_gather x1, waiting for transfers between devices, local(): whole_rows = lax.all_gather(mixed_rows, 'tp', axis=0, tiled=True)  11.7 us
    dot_general x1, matrix products, local(): jnp.einsum('tsecd,efd->tsecf', piece_rows, w_up, preferred_element_type=j...  11.4 us
    dot_general x1, matrix products, local(): jnp.einsum('tsecd,efd->tsecf', piece_rows, w_gate, preferred_element_type...  8.13 us
  transfers between devices with their start and end apart: 7, of which 6 were waited for; matrix products, arithmetic and copies ran while one was open for 3% of the time, Pallas kernels for 0%

profile of v1, /device:TPU:0, one launch (start us, length us, event | category | flops | bytes accessed | tf_op | source)
XLA Modules:
  0.0 318.7 jit_solution(9521204480455232224)
XLA Ops:
  7.7 4.9 %collective-permute-start = (bf16[128,128]{1,0:T(8,128)(2,1)S(1)}, bf16[128,128]{1,0:T(8,128)(2,1)S(1)}, u32[]{:S(2)}, u32[]{:S(2)}) collective-permute-start(bf16[128,128]{1,0:T(8,128)(2,1)S(1)} %get-tuple-element.10), channel_id=1, source_target_pairs={{0,4},{4,8},{8,12},{12,16},{16,20},{20,24},{24,28},{1,5},{5,9},{9,... | collective-permute-start | bytes 98312 | tf_op jit(solution)/shard_map/ppermute | solution.py:23
  12.6 1.3 collective-permute-start.1
  15.7 2.7 collective-permute-done.1
  20.4 1.8 fusion.27
  22.3 32.5 %reduce-scatter.2.cloned.1.call-done = f32[64,2048]{1,0:T(8,128)} async-done(((f32[256,2048]{1,0:T(8,128)}), f32[64,2048]{1,0:T(8,128)}) %reduce-scatter.2.cloned.1.call-update) | async-done | bytes 524304 | tf_op jit(solution)/shard_map/reduce_scatter | solution.py:97
  54.7 1.8 add_convert_fusion
  57.2 2.4 reduce-window.6
  60.4 1.3 convert_reduce_fusion
  61.7 11.7 %all-gather.6.cloned.1.call-done = bf16[256,2048]{1,0:T(8,128)(2,1)} async-done(((bf16[64,2048]{1,0:T(8,128)(2,1)}), bf16[256,2048]{1,0:T(8,128)(2,1)}) %all-gather.6.cloned.1.call-update) | async-done | bytes 1048592 | tf_op jit(solution)/shard_map/all_gather | solution.py:104
  73.4 1.5 multiply_reduce_fusion
  74.9 1.5 multiply_convert_fusion
  77.2 53.9 %all_to_all.14 = bf16[8,64,2048]{2,1,0:T(8,128)(2,1)S(1)} all-to-all(bf16[8,64,2048]{2,1,0:T(8,128)(2,1)S(1)} %bitcast.118), channel_id=1, replica_groups=mesh['sp'=8,'tp'=4] {'sp'}, dimensions={0} | all-to-all | bytes 4194304 | tf_op jit(solution)/shard_map/all_to_all | solution.py:122
  131.1 1.5 copy.71
  132.8 56.3 %all-gather.8.cloned.1.call-done = bf16[4,8,8,8,2048]{4,3,1,0,2:T(8,128)(2,1)} async-done(((bf16[1,8,8,8,2048]{4,3,1,0,2:T(8,128)(2,1)}), bf16[4,8,8,8,2048]{4,3,1,0,2:T(8,128)(2,1)}) %all-gather.8.cloned.1.call-update) | async-done | bytes 8388624 | tf_op jit(solution)/shard_map/all_gather | solution.py:124
  189.2 8.1 %fusion.4 = f32[8,4,8,8,256]{4,3,2,1,0:T(8,128)S(1)} fusion(bf16[4,8,8,8,2048]{4,3,1,0,2:T(8,128)(2,1)} %all-gather.8.cloned.1.call-done, bf16[8,256,2048]{2,1,0:T(8,128)(2,1)} %param.24), kind=kOutput, calls=%fused_computation.4 | convolution fusion | flops 2147483648 | bytes 18874368 | tf_op jit(solution)/shard_map/tsecd,efd->tsecf/dot_general | solution.py:125
  197.3 11.4 %fusion.6 = bf16[4,8,8,8,256]{4,3,1,0,2:T(8,128)(2,1)} fusion(f32[8,4,8,8,256]{4,3,2,1,0:T(8,128)S(1)} %fusion.4, bf16[4,8,8,8,2048]{4,3,1,0,2:T(8,128)(2,1)} %all-gather.8.cloned.1.call-done, bf16[8,256,2048]{2,1,0:T(8,128)(2,1)} %param.25), kind=kOutput, calls=%fused_computation.8 | convolution fusion | flops 2150629376 | bytes 19922944 | tf_op jit(solution)/shard_map/tsecd,efd->tsecf/dot_general | solution.py:128
  208.7 34.6 %all-gather.10.cloned.1.call-done = bf16[16,8,8,8,256]{4,3,1,0,2:T(8,128)(2,1)} async-done(((bf16[4,8,8,8,256]{4,3,1,0,2:T(8,128)(2,1)}), bf16[16,8,8,8,256]{4,3,1,0,2:T(8,128)(2,1)}) %all-gather.10.cloned.1.call-update) | async-done | bytes 4194320 | tf_op jit(solution)/shard_map/all_gather | solution.py:136
  243.3 2.7 copy.72
  246.0 5.8 %convert_bitcast_fusion = bf16[4,8,8,8,512]{4,3,1,0,2:T(8,128)(2,1)S(1)} fusion(bf16[4,8,8,8,1024]{4,3,1,0,2:T(8,128)(2,1)S(1)} %bitcast.122, bf16[8,1024,512]{2,1,0:T(8,128)(2,1)} %param.26), kind=kOutput, calls=%fused_computation.14 | convolution fusion | flops 2148532224 | bytes 14680064 | tf_op jit(solution)/shard_map/tsecf,efd->tsecd/dot_general | solution.py:140
  251.8 1.6 copy.73
  253.4 5.6 %all-to-all-start.1 = ((bf16[4,8,8,8,512]{4,3,0,2,1:T(8,128)(2,1)}), bf16[4,8,8,8,512]{4,3,0,2,1:T(8,128)(2,1)S(1)}, u32[]{:S(2)}, u32[]{:S(2)}) async-start(bf16[4,8,8,8,512]{4,3,0,2,1:T(8,128)(2,1)} %copy.73), calls=%async_computation.2 | async-start | bytes 4194304 | tf_op jit(solution)/shard_map/all_to_all | solution.py:146
  259.1 1.6 convert_element_type.61
  262.3 7.3 %all-gather.1 = bf16[256,1024]{1,0:T(8,128)(2,1)} all-gather(bf16[256,256]{1,0:T(8,128)(2,1)S(1)} %fusion.16), channel_id=3, replica_groups=mesh['sp'=8,'tp'=4] {'tp'}, dimensions={1}, use_global_device_ids=true | all-gather | bytes 655360 | tf_op jit(solution)/shard_map/all_gather | solution.py:138
  269.6 38.0 %all-to-all-done.1 = bf16[4,8,8,8,512]{4,3,0,2,1:T(8,128)(2,1)S(1)} async-done(((bf16[4,8,8,8,512]{4,3,0,2,1:T(8,128)(2,1)}), bf16[4,8,8,8,512]{4,3,0,2,1:T(8,128)(2,1)S(1)}, u32[]{:S(2)}, u32[]{:S(2)}) %all-to-all-start.1) | async-done | bytes 2097184 | tf_op jit(solution)/shard_map/all_to_all | solution.py:146
  (85 shorter events, 13.4 us)
Async XLA Ops:
  6.5 13.8 %copy-start = (bf16[256,2048]{1,0:T(8,128)(2,1)S(1)}, bf16[256,2048]{1,0:T(8,128)(2,1)}, u32[]{:S(2)}) copy-start(bf16[256,2048]{1,0:T(8,128)(2,1)} %param.19) | copy-start | bytes 3145732
  6.5 48.2 %reduce-scatter.2.cloned.1.call-start = ((), (), s32[]{:S(2)}) async-start(), calls=%async_computation.3 | async-start | bytes 2621440 | tf_op jit(solution)/shard_map/reduce_scatter | solution.py:97
  6.5 12.9 %copy-start.13 = (f32[4]{0:T(128)S(1)}, f32[4]{0:T(128)}, u32[]{:S(2)}) copy-start(f32[4]{0:T(128)} %param.18) | copy-start | bytes 52
  7.7 8.0 %collective-permute-start = (bf16[128,128]{1,0:T(8,128)(2,1)S(1)}, bf16[128,128]{1,0:T(8,128)(2,1)S(1)}, u32[]{:S(2)}, u32[]{:S(2)}) collective-permute-start(bf16[128,128]{1,0:T(8,128)(2,1)S(1)} %get-tuple-element.10), channel_id=1, source_target_pairs={{0,4},{4,8},{8,12},{12,16},{16,20},{20,24},{24,28},{1,5},{5,9},{9,... | collective-permute-start | bytes 98312 | tf_op jit(solution)/shard_map/ppermute | solution.py:23
  12.6 5.8 %collective-permute-start.1 = (bf16[128,128]{1,0:T(8,128)(2,1)S(1)}, bf16[128,128]{1,0:T(8,128)(2,1)S(1)}, u32[]{:S(2)}, u32[]{:S(2)}) collective-permute-start(bf16[128,128]{1,0:T(8,128)(2,1)S(1)} %get-tuple-element.11), channel_id=1, source_target_pairs={{4,0},{8,4},{12,8},{16,12},{20,16},{24,20},{28,24},{5,1},{9,5},{13... | collective-permute-start | bytes 98312 | tf_op jit(solution)/shard_map/ppermute | solution.py:24
  20.4 34.4 %copy-start.9 = (bf16[64,2048]{1,0:T(8,128)(2,1)S(1)}, bf16[64,2048]{1,0:T(8,128)(2,1)}, u32[]{:S(2)}) copy-start(bf16[64,2048]{1,0:T(8,128)(2,1)} %param.20) | copy-start | bytes 786436
  22.2 34.4 %copy-start.10 = (s32[256,4]{0,1:T(4,128)S(1)}, s32[256,4]{0,1:T(4,128)}, u32[]{:S(2)}) copy-start(s32[256,4]{0,1:T(4,128)} %param.22) | copy-start | bytes 12292
  22.2 38.1 %copy-start.11 = (f32[256,4]{0,1:T(4,128)S(1)}, f32[256,4]{0,1:T(4,128)}, u32[]{:S(2)}) copy-start(f32[256,4]{0,1:T(4,128)} %param.23) | copy-start | bytes 12292
  22.2 38.2 %copy-start.12 = (bf16[2048]{0:T(1024)(128)(2,1)S(1)}, bf16[2048]{0:T(1024)(128)(2,1)}, u32[]{:S(2)}) copy-start(bf16[2048]{0:T(1024)(128)(2,1)} %param.21) | copy-start | bytes 12292
  22.2 51.2 %all-gather.6.cloned.1.call-start = ((), (), s32[]{:S(2)}) async-start(), calls=%async_computation.4 | async-start | bytes 1310720 | tf_op jit(solution)/shard_map/all_gather | solution.py:104
  56.5 132.6 %all-gather.8.cloned.1.call-start = ((), (), s32[]{:S(2)}) async-start(), calls=%async_computation.5 | async-start | bytes 10485760 | tf_op jit(solution)/shard_map/all_gather | solution.py:124
  76.5 54.6 %copy-start.3 = (bf16[256,2048]{1,0:T(8,128)(2,1)}, bf16[256,2048]{1,0:T(8,128)(2,1)S(1)}, u32[]{:S(2)}) copy-start(bf16[256,2048]{1,0:T(8,128)(2,1)S(1)} %multiply_convert_fusion) | copy-start | bytes 3145732
  132.6 110.7 %all-gather.10.cloned.1.call-start = ((), (), s32[]{:S(2)}) async-start(), calls=%async_computation.6 | async-start | bytes 5242880 | tf_op jit(solution)/shard_map/all_gather | solution.py:136
  253.4 5.7 %copy-start.2 = (bf16[256,2048]{1,0:T(8,128)(2,1)S(1)}, bf16[256,2048]{1,0:T(8,128)(2,1)}, u32[]{:S(2)}) copy-start(bf16[256,2048]{1,0:T(8,128)(2,1)} %all-gather.6.cloned.1.call-done) | copy-start | bytes 3145732
  253.4 54.3 %all-to-all-start.1 = ((bf16[4,8,8,8,512]{4,3,0,2,1:T(8,128)(2,1)}), bf16[4,8,8,8,512]{4,3,0,2,1:T(8,128)(2,1)S(1)}, u32[]{:S(2)}, u32[]{:S(2)}) async-start(bf16[4,8,8,8,512]{4,3,0,2,1:T(8,128)(2,1)} %copy.73), calls=%async_computation.2 | async-start | bytes 4194304 | tf_op jit(solution)/shard_map/all_to_all | solution.py:146
  259.0 1.6 copy-start.4
  259.1 2.3 copy-start.7
  259.1 2.8 copy-start.14
  307.7 1.0 copy-start.6
  308.7 2.3 copy-start.5
  308.7 2.3 copy-start.8
  308.7 3.5 %copy-start.1 = (bf16[256,2048]{1,0:T(8,128)(2,1)S(1)}, bf16[256,2048]{1,0:T(8,128)(2,1)}, u32[]{:S(2)}) copy-start(bf16[256,2048]{1,0:T(8,128)(2,1)} %param.19) | copy-start | bytes 3145732
Sparse Core Ops, SparseCore 0:
  22.3 32.3 reduce-scatter.1
  56.7 16.6 all-gather.5
  132.7 56.3 all-gather.7
  208.8 34.4 all-gather.9
